TPU v7x, 512 devices: a whole 4x4x16 slice. The times are simulated.
512 devices in a mesh: ep: 32 (over z, core), tp: 16 (over y, x).
Axes of the slice: x: 4, y: 4, z: 16, core: 2. Of those that a mesh axis runs over, the one named last changes fastest.
Arguments:
- tokens: bfloat16 [4096, 2048], P('ep'), may hold values from -6 to 6
- cotangent: bfloat16 [4096, 2048], P('ep'), may hold values from -6 to 6
- expert_ids: int32 [4096, 2], P('ep'), may hold values from 0 to 31, all different within a row; in each aligned block of 128 rows (0 to 127, 128 to 255, ...) at most 16 rows name the same one
- route_weight: bfloat16 [4096, 2], P('ep'), may hold values from 0.19921875 to 1
- gate_weight: bfloat16 [32, 1024, 2048], P('ep', 'tp'), may hold values from -0.125 to 0.125
- up_weight: bfloat16 [32, 1024, 2048], P('ep', 'tp'), may hold values from -0.125 to 0.125
- down_weight: bfloat16 [32, 1024, 2048], P('ep', 'tp'), may hold values from -0.1875 to 0.1875
Outputs:
- tokens_grad: bfloat16 [4096, 2048], P('ep', 'tp')
- route_weight_grad: float32 [4096, 2], P('ep')
- gate_weight_grad: float32 [32, 1024, 2048], P('ep', 'tp')
- up_weight_grad: float32 [32, 1024, 2048], P('ep', 'tp')
- down_weight_grad: float32 [32, 1024, 2048], P('ep', 'tp')
Inputs may be any that keep to these rules, and one draw needn't show every extreme that they name: `expert_ids`: within each aligned block of 128 rows every expert is named at most 16 times; the two experts of a row differ.
All inputs are finite; a program needn't handle non-finite values.
Results may differ from a plain program's by a relative error of at most 0.0058.
Values may be sent and summed in bfloat16 or wider, within the bound.
A program may use at most 64 MiB of HBM per device.

v0:
```python
import math

import jax
import jax.numpy as jnp
from jax import lax
from jax.sharding import PartitionSpec as P


def sent_together(arrays, axis, split_dim, concat_dim, along):
    widths = [math.prod(a.shape[along:]) for a in arrays]
    both = jnp.concatenate(
        [a.reshape(*a.shape[:along], w) for a, w in zip(arrays, widths)], axis=along
    )
    out = lax.all_to_all(both, axis, split_axis=split_dim, concat_axis=concat_dim, tiled=True)
    pieces = jnp.split(out, [sum(widths[:k]) for k in range(1, len(widths))], axis=along)
    return tuple((b.reshape(*out.shape[:along], *a.shape[along:]) for a, b in zip(arrays, pieces)))


def sent_together_2(arrays, axis, dim, along):
    widths = [a.shape[along] for a in arrays]
    both = jnp.concatenate(arrays, axis=along)
    out = lax.all_gather(both, axis, axis=dim, tiled=True)
    return tuple(jnp.split(out, [sum(widths[:k]) for k in range(1, len(widths))], axis=along))


def copy_for_each(shard, axis):
    copies = jnp.broadcast_to(shard, (lax.axis_size(axis), *shard.shape))
    return lax.all_to_all(copies, axis, split_axis=0, concat_axis=0, tiled=True)


def of_everyone(shard, axis):
    everything = copy_for_each(shard, axis)
    return jnp.sum(everything, axis=0)


def gather_turned(arrays, axis, dims):
    turned = [jnp.moveaxis(a, dim, 0) for a, dim in zip(arrays, dims)]
    both = jnp.concatenate([t.reshape(len(t), -1) for t in turned], axis=1)
    out, at, gathered = (lax.all_gather(both, axis, axis=0, tiled=True), 0, [])
    for t, dim in zip(turned, dims):
        section = out[:, at : at + t[0].size].reshape(-1, *t.shape[1:])
        gathered.append(jnp.moveaxis(section, 0, dim))
        at += t[0].size
    return tuple(gathered)


def sent_together_3(arrays, axis, split_dim, concat_dim, along):
    both = jnp.concatenate(arrays, axis=along)
    out, at, gathered = (
        lax.all_to_all(both, axis, split_axis=split_dim, concat_axis=concat_dim, tiled=True),
        0,
        [],
    )
    for a in arrays:
        gathered.append(lax.slice_in_dim(out, at, at + a.shape[along], axis=along))
        at += a.shape[along]
    return tuple(gathered)


def per_device(tokens, cotangent, expert_ids, route_weight, gate_weight, up_weight, down_weight):
    tok_rows, model_width = tokens.shape
    top_count = expert_ids.shape[1]
    local_experts = gate_weight.shape[0]
    ep_size = lax.axis_size("ep")
    tp_size = lax.axis_size("tp")
    expert_count = local_experts * ep_size
    capacity = 2 * tok_rows * top_count // expert_count
    column_span = model_width // tp_size
    flat_ids = expert_ids.reshape(-1)
    routed = flat_ids.shape[0]
    member = (flat_ids[:, None] == jnp.arange(expert_count, dtype=jnp.int32)[None, :]).astype(
        jnp.int32
    )
    rank_slot = jnp.sum((jnp.cumsum(member, axis=0) - 1) * member, axis=1)
    slot_index = flat_ids * capacity + rank_slot
    buffer_rows = expert_count * capacity
    source_pair = (
        jnp.full((buffer_rows,), routed, jnp.int32)
        .at[slot_index]
        .set(jnp.arange(routed, dtype=jnp.int32))
    )
    filled = source_pair < routed
    safe_pair = jnp.minimum(source_pair, routed - 1)
    token_of = safe_pair // top_count
    zero_value = jnp.zeros((), tokens.dtype)
    send_weight = jnp.where(filled, route_weight.reshape(-1)[safe_pair], zero_value)
    offset = lax.axis_index("tp") * column_span
    token_cols = lax.dynamic_slice_in_dim(tokens, offset, column_span, 1)
    cotangent_cols = lax.dynamic_slice_in_dim(cotangent, offset, column_span, 1)
    part_tokens, part_cotangent, got_weight = sent_together(
        (token_cols[token_of], cotangent_cols[token_of], send_weight), "ep", 0, 0, 1
    )
    got_tokens, got_cotangent = sent_together_2((part_tokens, part_cotangent), "tp", 1, 0)
    block_shape = (ep_size, local_experts, capacity, model_width)
    routed_rows = got_tokens.reshape(block_shape)
    routed_cotangent = got_cotangent.reshape(block_shape)
    pair_weight = got_weight.reshape(ep_size, local_experts, capacity, 1).astype(jnp.float32)
    pre_gate = jnp.einsum(
        "secd,efd->secf", routed_rows, gate_weight, preferred_element_type=jnp.float32
    )
    pre_up = jnp.einsum(
        "secd,efd->secf", routed_rows, up_weight, preferred_element_type=jnp.float32
    )
    sigma = jax.nn.sigmoid(pre_gate)
    silu_gate = pre_gate * sigma
    hidden = silu_gate * pre_up
    back_hidden = jnp.einsum(
        "secd,efd->secf", routed_cotangent, down_weight, preferred_element_type=jnp.float32
    )
    pair_products = of_everyone(jnp.sum(hidden * back_hidden, axis=3), "tp")
    scaled = pair_weight * back_hidden
    grad_gate = (scaled * pre_up * sigma * (1.0 + pre_gate * (1.0 - sigma))).astype(jnp.bfloat16)
    grad_up = (scaled * silu_gate).astype(jnp.bfloat16)
    weighted = (pair_weight * hidden).astype(jnp.bfloat16)
    down_grad = jnp.einsum(
        "secf,secd->efd", weighted, routed_cotangent, preferred_element_type=jnp.float32
    )
    gate_grad = jnp.einsum(
        "secf,secd->efd", grad_gate, routed_rows, preferred_element_type=jnp.float32
    )
    up_grad = jnp.einsum("secf,secd->efd", grad_up, routed_rows, preferred_element_type=jnp.float32)
    full_gate, full_up = gather_turned((grad_gate, grad_up), "tp", (3, 3))
    gate_cols, up_cols = sent_together_3((gate_weight, up_weight), "tp", 2, 1, 0)
    pair_grad = (
        jnp.einsum("secf,efd->secd", full_gate, gate_cols, preferred_element_type=jnp.float32)
        + jnp.einsum("secf,efd->secd", full_up, up_cols, preferred_element_type=jnp.float32)
    ).astype(jnp.bfloat16)
    returned = lax.all_to_all(
        pair_grad.reshape(buffer_rows, column_span), "ep", split_axis=0, concat_axis=0, tiled=True
    )
    returned_products = lax.all_to_all(
        pair_products.reshape(buffer_rows), "ep", split_axis=0, concat_axis=0, tiled=True
    )
    per_pair = returned[slot_index].astype(jnp.float32).reshape(tok_rows, top_count, column_span)
    tokens_grad = jnp.sum(per_pair, axis=1).astype(jnp.bfloat16)
    route_grad = returned_products[slot_index].reshape(tok_rows, top_count)
    return (tokens_grad, route_grad, gate_grad, up_grad, down_grad)


def solution(mesh):
    in_specs = (
        P("ep", None),
        P("ep", None),
        P("ep", None),
        P("ep", None),
        P("ep", "tp", None),
        P("ep", "tp", None),
        P("ep", "tp", None),
    )
    out_specs = (
        P("ep", "tp"),
        P("ep", None),
        P("ep", "tp", None),
        P("ep", "tp", None),
        P("ep", "tp", None),
    )
    return jax.shard_map(
        per_device, mesh=mesh, in_specs=in_specs, out_specs=out_specs, check_vma=False
    )
```

profile of v0, /device:TPU:1, one launch (start us, length us, event | category | flops | bytes accessed | tf_op | source)
XLA Modules:
  0.0 244.9 jit_solution(12894059135491128948)
XLA Ops:
  7.2 0.7 broadcast_multiply_fusion
  7.9 0.8 copy.70
  9.0 0.8 copy.73
  11.2 1.4 scatter_custom_fusion
  12.6 3.4 %gather_fusion.2 = bf16[512]{0:T(512)(128)(2,1)S(1)} fusion(bf16[256]{0:T(256)(128)(2,1)S(1)} %reshape.200, s32[1024]{0:T(1024)S(1)} %get-tuple-element.38), kind=kCustom, calls=%fused_computation.2 | custom fusion | bytes 4096 | tf_op jit(solution)/shard_map/gather | solution.py:86
  16.0 0.8 constant_dynamic-slice_fusion
  16.8 1.3 gather_fusion.1
  18.1 1.3 gather_fusion
  19.8 44.3 %all_to_all.53 = bf16[32,16,257]{2,1,0:T(8,128)(2,1)S(1)} all-to-all(bf16[32,16,257]{2,1,0:T(8,128)(2,1)S(1)} %pad_maximum_fusion.1), channel_id=1, replica_groups=mesh['ep'=32,'tp'=16] {'ep'}, dimensions={0} | all-to-all | bytes 526336 | tf_op jit(solution)/shard_map/all_to_all | solution.py:14
  64.1 0.7 pad_maximum_fusion.2
  65.1 62.1 %all-gather.3.cloned.1.call-done = bf16[1024,2048]{1,0:T(8,128)(2,1)} async-done(((bf16[1024,128]{1,0:T(8,128)(2,1)}), bf16[1024,2048]{1,0:T(8,128)(2,1)}) %all-gather.3.cloned.1.call-update) | async-done | bytes 4194320 | tf_op jit(solution)/shard_map/all_gather | solution.py:22
  127.2 2.6 %fusion.49 = (bf16[512,2048]{1,0:T(8,128)(2,1)S(1)}, bf16[512,2048]{1,0:T(8,128)(2,1)S(1)}) fusion(bf16[1024,2048]{1,0:T(8,128)(2,1)} %all-gather.3.cloned.1.call-done), kind=kLoop, calls=%fused_computation.95 | loop fusion | bytes 8388608 | tf_op jit(solution)/shard_map/split | solution.py:23
  129.9 0.7 fusion.28
  131.0 0.7 fusion.26
  131.7 1.4 fusion.20
  133.3 0.6 pad_maximum_fusion.3
  134.0 0.8 pad_maximum_fusion
  134.8 2.3 copy.67
  137.2 1.5 reshape.290
  138.7 4.7 %all-to-all-start = ((bf16[16,2,8192]{2,1,0:T(2,128)(2,1)}), bf16[16,2,8192]{2,1,0:T(2,128)(2,1)}, u32[]{:S(2)}, u32[]{:S(2)}) async-start(bf16[16,2,8192]{2,1,0:T(2,128)(2,1)} %reshape.290), calls=%async_computation | async-start | bytes 1048576 | tf_op jit(solution)/shard_map/all_to_all | solution.py:50
  143.4 9.4 %all-to-all-done = bf16[16,2,8192]{2,1,0:T(2,128)(2,1)} async-done(((bf16[16,2,8192]{2,1,0:T(2,128)(2,1)}), bf16[16,2,8192]{2,1,0:T(2,128)(2,1)}, u32[]{:S(2)}, u32[]{:S(2)}) %all-to-all-start) | async-done | bytes 524320 | tf_op jit(solution)/shard_map/all_to_all | solution.py:50
  152.9 3.0 %reshape.291 = bf16[2048,2,64]{2,1,0:T(2,128)(2,1)S(1)} reshape(bf16[16,2,8192]{2,1,0:T(2,128)(2,1)} %all-to-all-done) | data formatting | bytes 1048576
  155.9 1.8 copy.68
  157.7 1.8 fusion.51
  159.6 1.3 fusion.10
  160.9 0.7 reshape.292
  161.7 3.5 %all-to-all-start.3 = ((f32[16,1,512]{2,1,0:T(1,128)}), f32[16,1,512]{2,1,0:T(1,128)S(1)}, u32[]{:S(2)}, u32[]{:S(2)}) async-start(f32[16,1,512]{2,1,0:T(1,128)} %reshape.292), calls=%async_computation.3 | async-start | bytes 65536 | tf_op jit(solution)/shard_map/all_to_all | solution.py:28
  165.2 3.0 %convolution_bitcast_fusion = f32[1,64,2048]{2,1,0:T(8,128)} fusion(bf16[32,16,2048]{2,1,0:T(8,128)(2,1)} %bitcast.214, f32[32,16]{1,0:T(8,128)S(1)} %reshape.217, f32[32,16,64]{2,1,0:T(8,128)S(1)} %copy-done.5, f32[32,16,64]{2,1,0:T(8,128)S(1)} %copy-done.6), kind=kOutput, calls=%fused_computation.6 | convolution fusion | flops 134447104 | bytes 2885632 | tf_op jit(solution)/shard_map/secf,secd->efd/dot_general | solution.py:115
  168.2 3.4 %all-to-all-done.3 = f32[16,1,512]{2,1,0:T(1,128)S(1)} async-done(((f32[16,1,512]{2,1,0:T(1,128)}), f32[16,1,512]{2,1,0:T(1,128)S(1)}, u32[]{:S(2)}, u32[]{:S(2)}) %all-to-all-start.3) | async-done | bytes 32800 | tf_op jit(solution)/shard_map/all_to_all | solution.py:28
  172.1 0.7 reduce.11
  172.9 0.7 copy.83
  173.6 16.6 %all-to-all-start.4 = ((f32[32,16,1]{1,2,0:T(1,128)}), f32[32,16,1]{1,2,0:T(1,128)S(1)}, u32[]{:S(2)}, u32[]{:S(2)}) async-start(f32[32,16,1]{1,2,0:T(1,128)} %copy.83), calls=%async_computation.4 | async-start | bytes 32768 | tf_op jit(solution)/shard_map/all_to_all | solution.py:131
  190.3 3.4 %all-gather.5.cloned.1.call-done = bf16[1024,1024]{1,0:T(8,128)(2,1)} async-done(((bf16[64,1024]{1,0:T(8,128)(2,1)}), bf16[1024,1024]{1,0:T(8,128)(2,1)}) %all-gather.5.cloned.1.call-update) | async-done | bytes 2097168 | tf_op jit(solution)/shard_map/all_gather | solution.py:39
  193.6 3.0 %fusion.50 = (bf16[1024,512]{1,0:T(8,128)(2,1)}, bf16[1024,512]{1,0:T(8,128)(2,1)}) fusion(bf16[1024,1024]{1,0:T(8,128)(2,1)} %all-gather.5.cloned.1.call-done), kind=kLoop, calls=%fused_computation.96 | loop fusion | bytes 4194304 | tf_op jit(solution)/shard_map/slice | solution.py:41
  196.6 2.3 copy.86
  198.9 2.3 copy.85
  201.2 2.1 fusion.3
  203.3 2.0 fusion.1
  205.3 0.7 copy.81
  206.0 14.6 %all-to-all-start.2 = ((bf16[32,16,128]{2,1,0:T(8,128)(2,1)}), bf16[32,16,128]{2,1,0:T(8,128)(2,1)S(1)}, u32[]{:S(2)}, u32[]{:S(2)}) async-start(bf16[32,16,128]{2,1,0:T(8,128)(2,1)} %copy.81), calls=%async_computation.2 | async-start | bytes 262144 | tf_op jit(solution)/shard_map/all_to_all | solution.py:128
  220.6 1.4 convolution_bitcast_fusion.1
  222.0 1.4 convolution_bitcast_fusion.2
  223.9 0.7 reduce.10
  224.7 1.9 gather_fusion.4
  226.8 0.6 copy.84
  227.4 9.0 %all-to-all-done.2 = bf16[32,16,128]{2,1,0:T(8,128)(2,1)S(1)} async-done(((bf16[32,16,128]{2,1,0:T(8,128)(2,1)}), bf16[32,16,128]{2,1,0:T(8,128)(2,1)S(1)}, u32[]{:S(2)}, u32[]{:S(2)}) %all-to-all-start.2) | async-done | bytes 131104 | tf_op jit(solution)/shard_map/all_to_all | solution.py:128
  236.4 0.9 gather_fusion.3
  237.3 0.8 reduce_sum.43
  (55 shorter events, 4.3 us)
Async XLA Ops:
  7.2 122.7 %copy-start = (bf16[1,64,2048]{2,1,0:T(8,128)(2,1)S(1)}, bf16[1,64,2048]{2,1,0:T(8,128)(2,1)}, u32[]{:S(2)}) copy-start(bf16[1,64,2048]{2,1,0:T(8,128)(2,1)} %param.13) | copy-start | bytes 786436
  7.2 120.0 %all-gather.3.cloned.1.call-start = ((), (), s32[]{:S(2)}) async-start(), calls=%async_computation.5 | async-start | bytes 4456448 | tf_op jit(solution)/shard_map/all_gather | solution.py:22
  64.9 128.8 %all-gather.5.cloned.1.call-start = ((), (), s32[]{:S(2)}) async-start(), calls=%async_computation.6 | async-start | bytes 2228224 | tf_op jit(solution)/shard_map/all_gather | solution.py:39
  129.8 1.9 copy-start.1
  129.8 1.1 copy-start.7
  129.9 1.8 copy-start.8
  130.6 2.5 %copy-start.2 = (f32[32,16,64]{2,1,0:T(8,128)}, f32[32,16,64]{2,1,0:T(8,128)S(1)}, u32[]{:S(2)}) copy-start(f32[32,16,64]{2,1,0:T(8,128)S(1)} %fusion.28) | copy-start | bytes 393220
  131.7 1.4 copy-start.4
  138.7 14.2 %all-to-all-start = ((bf16[16,2,8192]{2,1,0:T(2,128)(2,1)}), bf16[16,2,8192]{2,1,0:T(2,128)(2,1)}, u32[]{:S(2)}, u32[]{:S(2)}) async-start(bf16[16,2,8192]{2,1,0:T(2,128)(2,1)} %reshape.290), calls=%async_computation | async-start | bytes 1048576 | tf_op jit(solution)/shard_map/all_to_all | solution.py:50
  157.7 7.4 %copy-start.5 = (f32[32,16,64]{2,1,0:T(8,128)S(1)}, f32[32,16,64]{2,1,0:T(8,128)}, u32[]{:S(2)}) copy-start(f32[32,16,64]{2,1,0:T(8,128)} %copy-done.4) | copy-start | bytes 393220
  157.7 7.4 %copy-start.6 = (f32[32,16,64]{2,1,0:T(8,128)S(1)}, f32[32,16,64]{2,1,0:T(8,128)}, u32[]{:S(2)}) copy-start(f32[32,16,64]{2,1,0:T(8,128)} %get-tuple-element.37) | copy-start | bytes 393220
  161.7 9.9 %all-to-all-start.3 = ((f32[16,1,512]{2,1,0:T(1,128)}), f32[16,1,512]{2,1,0:T(1,128)S(1)}, u32[]{:S(2)}, u32[]{:S(2)}) async-start(f32[16,1,512]{2,1,0:T(1,128)} %reshape.292), calls=%async_computation.3 | async-start | bytes 65536 | tf_op jit(solution)/shard_map/all_to_all | solution.py:28
  173.6 32.4 %all-to-all-start.4 = ((f32[32,16,1]{1,2,0:T(1,128)}), f32[32,16,1]{1,2,0:T(1,128)S(1)}, u32[]{:S(2)}, u32[]{:S(2)}) async-start(f32[32,16,1]{1,2,0:T(1,128)} %copy.83), calls=%async_computation.4 | async-start | bytes 32768 | tf_op jit(solution)/shard_map/all_to_all | solution.py:131
  201.2 19.4 %copy-start.3 = (f32[32,16,64]{2,1,0:T(8,128)S(1)}, f32[32,16,64]{2,1,0:T(8,128)}, u32[]{:S(2)}) copy-start(f32[32,16,64]{2,1,0:T(8,128)} %copy-done.2) | copy-start | bytes 393220
  206.0 30.4 %all-to-all-start.2 = ((bf16[32,16,128]{2,1,0:T(8,128)(2,1)}), bf16[32,16,128]{2,1,0:T(8,128)(2,1)S(1)}, u32[]{:S(2)}, u32[]{:S(2)}) async-start(bf16[32,16,128]{2,1,0:T(8,128)(2,1)} %copy.81), calls=%async_computation.2 | async-start | bytes 262144 | tf_op jit(solution)/shard_map/all_to_all | solution.py:128
Sparse Core Ops, SparseCore 0:
  65.0 62.1 all-gather.2
  134.1 59.4 all-gather.4
where the time goes:
time: 246 us; the launch traced here: 245 us
  waiting for transfers between devices  87.4 us (36%)
  blocking collectives  44.3 us (18%)
  starting transfers between devices  39.5 us (16%)
  local copies, waits for them, and re-layouts  39.3 us (16%)
  between operations  14.4 us (6%)
  matrix products  12.7 us (5%)
  other arithmetic  7.35 us (3%)
    all_gather x1, waiting for transfers between devices, sent_together_2(): out = lax.all_gather(both, axis, axis=dim, tiled=True)  62.1 us
    all_to_all x1, blocking collectives, sent_together(): lax.all_to_all(both, axis, split_axis=split_dim, concat_axis=concat_dim,...  44.3 us
    all_to_all x1, starting transfers between devices, per_device(): lax.all_to_all(pair_products.reshape(buffer_rows), 'ep', split_axis=0, co...  16.6 us
    all_to_all x1, starting transfers between devices, per_device(): lax.all_to_all(pair_grad.reshape(buffer_rows, column_span), 'ep', split_a...  14.6 us
    unnamed x28, local copies, waits for them, and re-layouts  12.6 us
    all_to_all x1, waiting for transfers between devices, sent_together_3(): lax.all_to_all(both, axis, split_axis=split_dim, concat_axis=concat_dim,...  9.45 us
    all_to_all x1, waiting for transfers between devices, per_device(): lax.all_to_all(pair_grad.reshape(buffer_rows, column_span), 'ep', split_a...  9 us
  transfers between devices with their start and end apart: 6, of which 5 were waited for; matrix products, arithmetic and copies ran while one was open for 15% of the time, Pallas kernels for 0%

commit v1 on v0

v1 whole, which is shorter than its diff:
```python
import functools

import jax
import jax.numpy as jnp
from jax import lax
from jax.experimental import pallas as pl
from jax.experimental.pallas import tpu as pltpu
from jax.sharding import PartitionSpec as P

MESH = pl.DeviceIdType.MESH
F32, BF16 = jnp.float32, jnp.bfloat16
CAP = 16
LANES = 128
CHUNKS = 4


def dot(a, b, dims=((1,), (0,))):
    return lax.dot_general(a, b, (dims, ((), ())), preferred_element_type=F32)


def kernel(nz, side, tok, cot, ids_ref, rw_ref, gw, uw, dw, tg_out, rg_out, gg_out, ug_out, dg_out,
           tokc, cotc, wgu, wd, send, rows, wx, wy, gsrc, grecv, ght, hht, pkeep, psrc, precv,
           pback, q0, q1r, q1s, q2r, qtot, ret, retq, ggv, ugv, dgv,
           sem_tc, sem_w, sem_wd, sem_out, s_a, r_a, s_b, r_b, s_w, r_w, s_g, r_g, s_p, r_p,
           s_q1, r_q1, s_q2, r_q2, s_e, r_e, s_f, r_f):
    n_ep, n_tp = 2 * nz, side * side
    slots = n_ep
    per = slots // CHUNKS
    sub = per // 2
    crows = per * CAP
    me, mt = lax.axis_index("ep"), lax.axis_index("tp")
    z, core = me // 2, lax.rem(me, 2)
    y, x = mt // side, lax.rem(mt, side)

    def at(dx, dy):
        return lax.rem(y + dy, side) * side + lax.rem(x + dx, side)

    def along(axis, d):
        return at(d, 0) if axis == 0 else at(0, d)

    def far(slot):
        i, rc = slot // 2, slot % 2
        d = (i + 1) // 2 if i % 2 else (nz - i // 2) % nz
        return lax.rem(z + d, nz) * 2 + lax.rem(core + rc, 2)

    def back_slot(slot):
        i, rc = slot // 2, slot % 2
        if 0 < i < nz - 1:
            i = i + 1 if i % 2 else i - 1
        return 2 * i + rc

    def rcopy(src, dst, ssem, rsem, ep, tp):
        return pltpu.make_async_remote_copy(
            src_ref=src, dst_ref=dst, send_sem=ssem, recv_sem=rsem,
            device_id={"ep": ep, "tp": tp}, device_id_type=MESH,
        )

    def got(ref, rsem):
        pltpu.make_async_copy(ref, ref, rsem).wait()

    barrier = pltpu.get_barrier_semaphore()

    def greet(i, carry):
        pl.semaphore_signal(barrier, inc=1, device_id={"ep": lax.rem(me + i, n_ep), "tp": mt}, device_id_type=MESH)
        return carry

    lax.fori_loop(1, n_ep, greet, 0)
    for d in range(1, side):
        for axis in range(2):
            pl.semaphore_signal(barrier, inc=1, device_id={"ep": me, "tp": along(axis, d)}, device_id_type=MESH)

    col = pl.ds(pl.multiple_of(mt * LANES, LANES), LANES)
    load_t = pltpu.make_async_copy(tok.at[:, col], tokc, sem_tc.at[0])
    load_c = pltpu.make_async_copy(cot.at[:, col], cotc, sem_tc.at[1])
    load_t.start()
    load_c.start()
    fh = gw.shape[1]

    for b in range(n_tp):
        cols = pl.ds(b * LANES, LANES)
        pltpu.make_async_copy(gw.at[0, :, cols], wgu.at[b, pl.ds(0, fh)], sem_w).start()
        pltpu.make_async_copy(uw.at[0, :, cols], wgu.at[b, pl.ds(fh, fh)], sem_w).start()
        for h in range(2):
            pltpu.make_async_copy(dw.at[0, :, cols], wd.at[b, pl.ds(h * fh, fh)], sem_wd).start()

    nt = tokc.shape[0]
    lane = lax.broadcasted_iota(jnp.int32, (nt, LANES), 1)
    row = lax.broadcasted_iota(jnp.int32, (nt, LANES), 0)
    ids = [ids_ref[:, k : k + 1] for k in range(2)]
    wt = [rw_ref[:, k : k + 1].astype(F32) for k in range(2)]
    mem = [(lane == ids[k]).astype(F32) for k in range(2)]
    lower = (lane < row).astype(BF16)
    before = dot(lower, (mem[0] + mem[1]).astype(BF16))
    rank = [jnp.sum(mem[k] * before, axis=1, keepdims=True).astype(jnp.int32) for k in range(2)]
    wide = lax.broadcasted_iota(jnp.int32, (nt, n_ep * CAP), 1)
    hot = [(wide == ids[k] * CAP + rank[k]).astype(F32) for k in range(2)]
    pick = hot[0] + hot[1]
    scaled = hot[0] * wt[0] + hot[1] * wt[1]
    pick_t = jnp.transpose(pick).astype(BF16)
    scaled_t = jnp.transpose(scaled).astype(BF16)
    load_t.wait()
    load_c.wait()
    send[:, 0] = dot(pick_t, tokc[...]).astype(BF16).reshape(n_ep, CAP, LANES)
    send[:, 1] = dot(scaled_t, cotc[...]).astype(BF16).reshape(n_ep, CAP, LANES)
    rows[mt, 0] = send[me]
    got(wgu, sem_w)
    got(wd, sem_wd)

    pl.semaphore_wait(barrier, n_ep - 1 + 2 * (side - 1))

    for s in range(1, slots):
        b = back_slot(s)
        e = far(s)
        rcopy(send.at[e], rows.at[mt, b], s_a, r_a.at[b // per], e, mt).start()
    for d in range(1, side):
        rcopy(wgu.reshape(side, side, LANES, LANES).at[:, lax.rem(x + d, side)], wx.at[side - d], s_w.at[0], r_w.at[0], me, along(0, d)).start()
        rcopy(wgu.reshape(side, side, LANES, LANES).at[lax.rem(y + d, side)], wy.at[side - d], s_w.at[1], r_w.at[1], me, along(1, d)).start()

    def place(axis, du, dv):
        return at(du, dv) if axis == 0 else at(dv, du)

    def pass_on(q, du, dv, second, step):
        axis = q % 2
        ref = rows.at[place(axis, du, dv), pl.ds(q * sub, sub)]
        rdu, rdv = (du, (dv - step) % side) if second else ((du - step) % side, dv)
        peer = along(1 - axis if second else axis, step % side)
        rcopy(ref, ref, s_b, r_b.at[(q * side + rdu) * side + rdv], me, peer).start()

    def block(q, du, dv):
        ref = rows.at[place(q % 2, du, dv), pl.ds(q * sub, sub)]
        got(ref, r_b.at[(q * side + du) * side + dv])

    def both(q, du, dv, second):
        pass_on(q, du, dv, second, 1)
        pass_on(q, du, dv, second, -1)

    def relay(q, keep, second):
        v = side - 1 if (q // 2) % 2 == 0 else 1
        step = 1 if v == side - 1 else -1
        pass_on(q, *((keep, v) if second else (v, keep)), second, step)

    def level0(g):
        if g == 0:
            got(rows.at[mt, pl.ds(1, per - 1)], r_a.at[0])
        else:
            got(rows.at[mt, pl.ds(g * per, per)], r_a.at[g])
        for q in (2 * g, 2 * g + 1):
            both(q, 0, 0, False)
            both(q, 0, 0, True)

    def second_in(q, du):
        block(q, du, 1)
        block(q, du, side - 1)
        relay(q, du, True)

    def level1(g):
        for q in (2 * g, 2 * g + 1):
            block(q, 1, 0)
            block(q, side - 1, 0)
            relay(q, 0, False)
            both(q, 1, 0, True)
            both(q, side - 1, 0, True)
        for q in (2 * g, 2 * g + 1):
            second_in(q, 0)

    def level2(g):
        for q in (2 * g, 2 * g + 1):
            block(q, 2, 0)
            both(q, 2, 0, True)
        for q in (2 * g, 2 * g + 1):
            second_in(q, 1)
            second_in(q, side - 1)

    def level3(g):
        for q in (2 * g, 2 * g + 1):
            second_in(q, 2)

    def level4(g):
        for q in (2 * g, 2 * g + 1):
            for du in range(side):
                block(q, du, 2)

    half = lax.broadcasted_iota(jnp.int32, (crows, LANES), 1) < fh

    def level5(g):
        pre = jnp.zeros((crows, LANES), F32)
        back = jnp.zeros((crows, LANES), F32)
        for b in range(0, n_tp, 2):
            a = [rows[b + i, pl.ds(g * per, per)] for i in range(2)]
            t = jnp.concatenate([a[i][:, 0].reshape(crows, LANES) for i in range(2)], axis=1)
            c = jnp.concatenate([a[i][:, 1].reshape(crows, LANES) for i in range(2)], axis=1)
            wt_b = jnp.concatenate([wgu[b], wgu[b + 1]], axis=1)
            wd_b = jnp.concatenate([wd[b], wd[b + 1]], axis=1)
            pre = pre + dot(t, wt_b, ((1,), (1,)))
            back = back + dot(c, wd_b, ((1,), (1,)))
        other = pltpu.roll(pre, fh, 1)
        gate = jnp.where(half, pre, other)
        up = jnp.where(half, other, pre)
        sig = jax.nn.sigmoid(gate)
        silu = gate * sig
        hidden = silu * up
        grad = back * jnp.where(half, up * sig * (1.0 + gate * (1.0 - sig)), silu)
        gsrc[g] = grad.astype(BF16)
        ght[:, g * crows : (g + 1) * crows] = jnp.transpose(grad).astype(BF16)
        hht[:, g * crows : (g + 1) * crows] = jnp.transpose(hidden)[:fh].astype(BF16)
        prod = jnp.transpose(jnp.where(half, hidden * back, 0.0))
        q0[g] = jnp.sum(prod, axis=0, keepdims=True)
        axis = g % 2
        for d in range(1, side):
            rcopy(gsrc.at[g], grecv.at[g, side - d], s_g, r_g.at[g], me, along(axis, d)).start()
        for d in range(1, side):
            rcopy(q0.at[g], q1r.at[g, side - d], s_q1, r_q1.at[g], me, along(0, d)).start()

    def level6(g):
        axis = g % 2
        if g < 2:
            got((wx if axis == 0 else wy).at[pl.ds(1, side - 1)], r_w.at[axis])
        got(grecv.at[g, pl.ds(1, side - 1)], r_g.at[g])
        wr = wx if axis == 0 else wy
        spot = y if axis == 0 else x
        lhs = [gsrc[g]] + [grecv[g, r] for r in range(1, side)]
        lhs = [jnp.concatenate(lhs[k : k + 2], axis=1) for k in range(0, side, 2)]
        for d in range(0, side, 2):
            acc = jnp.zeros((crows, 2 * LANES), F32)
            for k in range(0, side, 2):
                parts = []
                for r in (k, k + 1):
                    w = []
                    for dd in (d, d + 1):
                        w.append(wgu[along(1 - axis, dd)] if r == 0 else wr[r, lax.rem(spot + dd, side)])
                    parts.append(jnp.concatenate(w, axis=1))
                acc = acc + dot(lhs[k // 2], jnp.concatenate(parts, axis=0))
            for i, dd in enumerate((d, d + 1)):
                piece = acc[:, i * LANES : (i + 1) * LANES]
                if dd == 0:
                    pkeep[g] = piece
                else:
                    psrc[g, dd] = piece.astype(BF16)
        for d in range(1, side):
            rcopy(psrc.at[g, d], precv.at[g, side - d], s_p, r_p.at[g], me, along(1 - axis, d)).start()
        got(q1r.at[g, pl.ds(1, side - 1)], r_q1.at[g])
        q1s[g] = q0[g] + q1r[g, 1] + q1r[g, 2] + q1r[g, 3]
        for d in range(1, side):
            rcopy(q1s.at[g], q2r.at[g, side - d], s_q2, r_q2.at[g], me, along(1, d)).start()

    def level7(g):
        got(precv.at[g, pl.ds(1, side - 1)], r_p.at[g])
        total = pkeep[g]
        for r in range(1, side):
            total = total + precv[g, r].astype(F32)
        pback[g] = total.astype(BF16).reshape(per, CAP, LANES)
        got(q2r.at[g, pl.ds(1, side - 1)], r_q2.at[g])
        qtot[g] = q1s[g] + q2r[g, 1] + q2r[g, 2] + q2r[g, 3]
        for i in range(per):
            s = g * per + i
            if s == 0:
                ret[me] = pback[0, 0]
                retq[me] = qtot[0]
            else:
                e = far(s)
                rcopy(pback.at[g, i], ret.at[me], s_e, r_e, e, mt).start()
                rcopy(qtot.at[g], retq.at[me], s_f, r_f, e, mt).start()

    def weight_grads(which):
        outs = []
        for b in range(0, n_tp, 2):
            c = jnp.concatenate([rows[b + i, :, which].reshape(slots * CAP, LANES) for i in range(2)], axis=1)
            cols = slice(b * LANES, (b + 2) * LANES)
            if which == 0:
                r = dot(ght[...], c)
                ggv[0, :, cols] = r[:fh]
                ugv[0, :, cols] = r[fh:]
            else:
                dgv[0, :, cols] = dot(hht[...], c)
        pairs = ((ggv, gg_out, 0), (ugv, ug_out, 1)) if which == 0 else ((dgv, dg_out, 2),)
        for src, dst, k in pairs:
            copy = pltpu.make_async_copy(src, dst, sem_out.at[k])
            copy.start()
            outs.append(copy)
        return outs

    levels = [level0, level1, level2, level3, level4, level5, level6, level7]
    outs = []
    for t in range(CHUNKS + len(levels) - 1):
        for k in reversed(range(len(levels))):
            if 0 <= t - k < CHUNKS:
                levels[k](t - k)
        if t == CHUNKS + 4:
            outs += weight_grads(0)
        if t == CHUNKS + 6:
            outs += weight_grads(1)

    got(ret.at[pl.ds(0, n_ep - 1)], r_e)
    tg_out[...] = dot(pick.astype(BF16), ret[...].reshape(n_ep * CAP, LANES)).astype(BF16)
    got(retq.at[pl.ds(0, n_ep - 1)], r_f)
    cols = []
    for k in range(2):
        e_z, e_core = ids[k] // 2, lax.rem(ids[k], 2)
        d = lax.rem(z - e_z + nz, nz)
        i = jnp.where(d == 0, 0, jnp.where(d <= nz // 2, 2 * d - 1, 2 * (nz - d)))
        s = 2 * i + lax.rem(core + e_core, 2)
        want = lax.rem(s, per) * CAP + rank[k]
        acc = jnp.zeros((nt, LANES), F32)
        for e in range(n_ep):
            acc = jnp.where(ids[k] == e, retq[e], acc)
        acc = jnp.sum(jnp.where(lane == want, acc, 0.0), axis=1, keepdims=True)
        cols.append(acc / wt[k])
    rg_out[...] = jnp.concatenate(cols, axis=1)

    got(send.at[pl.ds(0, n_ep - 1)], s_a)
    got(rows.at[pl.ds(0, n_tp - 1)], s_b)
    got(wx.at[pl.ds(1, side - 1)], s_w.at[0])
    got(wy.at[pl.ds(1, side - 1)], s_w.at[1])
    got(grecv.at[:, pl.ds(1, side - 1)], s_g)
    got(precv.at[:, pl.ds(1, side - 1)], s_p)
    got(q1r.at[:, pl.ds(1, side - 1)], s_q1)
    got(q2r.at[:, pl.ds(1, side - 1)], s_q2)
    got(ret.at[pl.ds(0, n_ep - 1)], s_e)
    got(retq.at[pl.ds(0, n_ep - 1)], s_f)
    for copy in outs:
        copy.wait()


def per_device(nz, side, tokens, cotangent, expert_ids, route_weight, gate_weight, up_weight, down_weight):
    n_ep, n_tp = 2 * nz, side * side
    per = n_ep // CHUNKS
    crows = per * CAP
    nt, width = tokens.shape
    fh = gate_weight.shape[1]
    vmem = pl.BlockSpec(memory_space=pltpu.VMEM)
    hbm = pl.BlockSpec(memory_space=pl.ANY)
    wshape = jax.ShapeDtypeStruct(gate_weight.shape, F32)
    dma = pltpu.SemaphoreType.DMA
    scratch = [
        pltpu.VMEM((nt, LANES), BF16),
        pltpu.VMEM((nt, LANES), BF16),
        pltpu.VMEM((n_tp, LANES, LANES), BF16),
        pltpu.VMEM((n_tp, LANES, LANES), BF16),
        pltpu.VMEM((n_ep, 2, CAP, LANES), BF16),
        pltpu.VMEM((n_tp, n_ep, 2, CAP, LANES), BF16),
        pltpu.VMEM((side, side, LANES, LANES), BF16),
        pltpu.VMEM((side, side, LANES, LANES), BF16),
        pltpu.VMEM((CHUNKS, crows, LANES), BF16),
        pltpu.VMEM((CHUNKS, side, crows, LANES), BF16),
        pltpu.VMEM((LANES, n_ep * CAP), BF16),
        pltpu.VMEM((fh, n_ep * CAP), BF16),
        pltpu.VMEM((CHUNKS, crows, LANES), F32),
        pltpu.VMEM((CHUNKS, side, crows, LANES), BF16),
        pltpu.VMEM((CHUNKS, side, crows, LANES), BF16),
        pltpu.VMEM((CHUNKS, per, CAP, LANES), BF16),
        pltpu.VMEM((CHUNKS, 1, LANES), F32),
        pltpu.VMEM((CHUNKS, side, 1, LANES), F32),
        pltpu.VMEM((CHUNKS, 1, LANES), F32),
        pltpu.VMEM((CHUNKS, side, 1, LANES), F32),
        pltpu.VMEM((CHUNKS, 1, LANES), F32),
        pltpu.VMEM((n_ep, CAP, LANES), BF16),
        pltpu.VMEM((n_ep, 1, LANES), F32),
        pltpu.VMEM(gate_weight.shape, F32),
        pltpu.VMEM(gate_weight.shape, F32),
        pltpu.VMEM(gate_weight.shape, F32),
        dma((2,)), dma, dma, dma((3,)),
        dma, dma((CHUNKS,)),
        dma, dma((2 * CHUNKS * n_tp,)),
        dma((2,)), dma((2,)),
        dma, dma((CHUNKS,)),
        dma, dma((CHUNKS,)),
        dma, dma((CHUNKS,)),
        dma, dma((CHUNKS,)),
        dma, dma,
        dma, dma,
    ]
    return tuple(pl.pallas_call(
        functools.partial(kernel, nz, side),
        out_shape=(
            jax.ShapeDtypeStruct((nt, LANES), BF16),
            jax.ShapeDtypeStruct((nt, 2), F32),
            wshape, wshape, wshape,
        ),
        in_specs=[hbm, hbm, vmem, vmem, hbm, hbm, hbm],
        out_specs=(vmem, vmem, hbm, hbm, hbm),
        scratch_shapes=scratch,
        compiler_params=pltpu.CompilerParams(collective_id=0, has_side_effects=True, vmem_limit_bytes=48 * 1024 * 1024),
    )(tokens, cotangent, expert_ids, route_weight, gate_weight, up_weight, down_weight))


def solution(mesh):
    nz = mesh.shape["ep"] // 2
    side = 4
    in_specs = (
        P("ep", None), P("ep", None), P("ep", None), P("ep", None),
        P("ep", "tp", None), P("ep", "tp", None), P("ep", "tp", None),
    )
    out_specs = (
        P("ep", "tp"), P("ep", None), P("ep", "tp", None), P("ep", "tp", None), P("ep", "tp", None),
    )
    return jax.shard_map(
        functools.partial(per_device, nz, side), mesh=mesh, in_specs=in_specs, out_specs=out_specs, check_vma=False
    )
```

time: 246 us -> 91 us (0.37)
  waiting for transfers between devices: 87.4 us -> 0 us
  Pallas kernels: 0 us -> 80.6 us
  blocking collectives: 44.3 us -> 0 us
  starting transfers between devices: 39.5 us -> 0 us
  local copies, waits for them, and re-layouts: 39.3 us -> 9.46 us
  between operations: 14.4 us -> 0.66 us
  matrix products: 12.7 us -> 0 us
  other arithmetic: 7.35 us -> 0 us
    pallas_call x0 -> x1, Pallas kernels: none -> 80.6 us  [per_device(): pl.pallas_call(functools.partial(kernel, nz, side), out_shape=(jax.ShapeD...]
    all_gather x2 -> x0, waiting for transfers between devices: 65.5 us -> none  [the longest x1 62.1 us: sent_together_2(): out = lax.all_gather(both, axis, axis=dim, tiled=True)]
    all_to_all x1 -> x0, blocking collectives: 44.3 us -> none  [sent_together(): lax.all_to_all(both, axis, split_axis=split_dim, concat_axis=concat_dim,...]
    all_to_all x4 -> x0, starting transfers between devices: 39.4 us -> none  [the longest x1 16.6 us: per_device(): lax.all_to_all(pair_products.reshape(buffer_rows), 'ep', split_axis=0, co...]
    all_to_all x4 -> x0, waiting for transfers between devices: 21.8 us -> none  [the longest x1 9.45 us: sent_together_3(): lax.all_to_all(both, axis, split_axis=split_dim, concat_axis=concat_dim,...]
    dot_general x8 -> x0, matrix products: 12.7 us -> none  [the longest x1 2.98 us: per_device(): jnp.einsum('secf,secd->efd', weighted, routed_cotangent, preferred_elemen...]
    gather x5 -> x0, local copies, waits for them, and re-layouts: 8.83 us -> none  [the longest x1 3.36 us: per_device(): route_weight.reshape(-1)[safe_pair]]
    slice x3 -> x0, local copies, waits for them, and re-layouts: 4.98 us -> none  [the longest x1 2.97 us: gather_turned(): section = out[:, at:at + t[0].size].reshape(-1, *t.shape[1:])]
  transfers between devices with their start and end apart: 6 -> 0, of which waited for: 5 -> 0; matrix products, arithmetic and copies ran while one was open for 15% -> 0% of each run, Pallas kernels for 0% -> 0%
where the time goes in v1:
time: 91 us; the launch traced here: 90.7 us
  Pallas kernels  80.6 us (89%)
  local copies, waits for them, and re-layouts  9.46 us (10%)
    pallas_call x1, Pallas kernels, per_device(): pl.pallas_call(functools.partial(kernel, nz, side), out_shape=(jax.ShapeD...  80.6 us
    unnamed x18, local copies, waits for them, and re-layouts  8.83 us

profile of v1, /device:TPU:1, one launch (start us, length us, event | category | flops | bytes accessed | tf_op | source)
XLA Modules:
  0.0 90.7 jit_solution(10879522485398441456)
XLA Ops:
  0.6 0.0 copy-start.5
  0.6 0.8 copy.13.rw_ref
  1.4 0.0 copy-done.5
  1.4 0.1 copy.12.ids_ref
  1.5 0.0 copy-start
  1.6 1.0 %copy-done = bf16[128,2048]{1,0:T(8,128)(2,1)S(1)} copy-done((bf16[128,2048]{1,0:T(8,128)(2,1)S(1)}, bf16[128,2048]{1,0:T(8,128)(2,1)}, u32[]{:S(2)}) %copy-start) | copy-done | bytes 524312
  2.6 0.0 copy-start.1
  2.6 1.0 %copy-done.1 = bf16[128,2048]{1,0:T(8,128)(2,1)S(1)} copy-done((bf16[128,2048]{1,0:T(8,128)(2,1)S(1)}, bf16[128,2048]{1,0:T(8,128)(2,1)}, u32[]{:S(2)}) %copy-start.1) | copy-done | bytes 524312
  3.6 0.0 copy-start.2
  3.6 0.9 %copy-done.2 = bf16[1,64,2048]{2,1,0:T(8,128)(2,1)S(1)} copy-done((bf16[1,64,2048]{2,1,0:T(8,128)(2,1)S(1)}, bf16[1,64,2048]{2,1,0:T(8,128)(2,1)}, u32[]{:S(2)}) %copy-start.2) | copy-done | bytes 262168
  4.6 0.0 copy-start.3
  4.6 0.9 %copy-done.3 = bf16[1,64,2048]{2,1,0:T(8,128)(2,1)S(1)} copy-done((bf16[1,64,2048]{2,1,0:T(8,128)(2,1)S(1)}, bf16[1,64,2048]{2,1,0:T(8,128)(2,1)}, u32[]{:S(2)}) %copy-start.3) | copy-done | bytes 262168
  5.5 0.0 copy-start.4
  5.5 0.9 %copy-done.4 = bf16[1,64,2048]{2,1,0:T(8,128)(2,1)S(1)} copy-done((bf16[1,64,2048]{2,1,0:T(8,128)(2,1)S(1)}, bf16[1,64,2048]{2,1,0:T(8,128)(2,1)}, u32[]{:S(2)}) %copy-start.4) | copy-done | bytes 262168
  6.5 80.6 %shard_map.110 = (bf16[128,128]{1,0:T(8,128)(2,1)S(1)}, f32[128,2]{1,0:T(8,128)S(1)}, f32[1,64,2048]{2,1,0:T(8,128)S(1)}, f32[1,64,2048]{2,1,0:T(8,128)S(1)}, f32[1,64,2048]{2,1,0:T(8,128)S(1)}) custom-call(bf16[128,2048]{1,0:T(8,128)(2,1)S(1)} %copy-done, bf16[128,2048]{1,0:T(8,128)(2,1)S(1)} %copy-done.1, s32[128,2]{1,0:T(8,128)S(1)} %copy.12.ids_ref, ...), custom_call_target="tpu_custom_call" | custom-call | tf_op jit(solution)/shard_map/pallas_call | solution.py:372
  87.1 0.6 copy.14
  87.7 0.6 copy.19
  88.3 0.8 copy.20
  89.1 0.8 copy.21
  89.9 0.8 copy.22
Async XLA Ops:
  0.6 0.8 copy-start.5
  1.5 1.0 %copy-start = (bf16[128,2048]{1,0:T(8,128)(2,1)S(1)}, bf16[128,2048]{1,0:T(8,128)(2,1)}, u32[]{:S(2)}) copy-start(bf16[128,2048]{1,0:T(8,128)(2,1)} %tok.1) | copy-start | bytes 1572868
  2.6 1.0 %copy-start.1 = (bf16[128,2048]{1,0:T(8,128)(2,1)S(1)}, bf16[128,2048]{1,0:T(8,128)(2,1)}, u32[]{:S(2)}) copy-start(bf16[128,2048]{1,0:T(8,128)(2,1)} %cot.1) | copy-start | bytes 1572868
  3.6 0.9 %copy-start.2 = (bf16[1,64,2048]{2,1,0:T(8,128)(2,1)S(1)}, bf16[1,64,2048]{2,1,0:T(8,128)(2,1)}, u32[]{:S(2)}) copy-start(bf16[1,64,2048]{2,1,0:T(8,128)(2,1)} %gw.1) | copy-start | bytes 786436
  4.6 0.9 %copy-start.3 = (bf16[1,64,2048]{2,1,0:T(8,128)(2,1)S(1)}, bf16[1,64,2048]{2,1,0:T(8,128)(2,1)}, u32[]{:S(2)}) copy-start(bf16[1,64,2048]{2,1,0:T(8,128)(2,1)} %uw.1) | copy-start | bytes 786436
  5.5 0.9 %copy-start.4 = (bf16[1,64,2048]{2,1,0:T(8,128)(2,1)S(1)}, bf16[1,64,2048]{2,1,0:T(8,128)(2,1)}, u32[]{:S(2)}) copy-start(bf16[1,64,2048]{2,1,0:T(8,128)(2,1)} %dw.1) | copy-start | bytes 786436

commit v2 on v1

v2 whole, which is shorter than its diff:
```python
import functools

import jax
import jax.numpy as jnp
from jax import lax
from jax.experimental import pallas as pl
from jax.experimental.pallas import tpu as pltpu
from jax.sharding import PartitionSpec as P

MESH = pl.DeviceIdType.MESH
F32, BF16 = jnp.float32, jnp.bfloat16
CAP = 16
LANES = 128
SIZES = (8, 8, 8, 8)
CHUNKS = len(SIZES)
START = tuple(sum(SIZES[:g]) for g in range(CHUNKS))
SIDE = 4


def dot(a, b, dims=((1,), (0,)), **kw):
    return lax.dot_general(a, b, (dims, ((), ())), preferred_element_type=F32, **kw)


def slot_order(nz):
    near = [0] + [d for k in range(1, nz // 2) for d in (k, nz - k)] + [nz // 2]
    n = nz // 4
    return near[:n] + near[2 * n :] + near[n : 2 * n]


FIRST_AXIS = (0, 1) * CHUNKS
FIRST_STEP = (1, 1, -1, -1) * CHUNKS
DIRECT1 = tuple(range(2 * CHUNKS))
DIRECT2 = ()
WEIGHTS_AT = -1
AHEAD = 0


def kernel(nz, tok, cot, ids_hbm, rw_hbm, gw, uw, dw, tg_out, rg_out, gg_out, ug_out, dg_out,
           ids_ref, rw_ref, tokc, cotc, wgu, wd, send, rows, wx, gsrc, hsrc, grecv, pkeep, psrc, precv,
           pback, q0, q1r, q1s, q2r, qsend, ret, retq, pickv,
           sem_i, sem_tc, sem_w, sem_wd, s_a, r_a, s_b, r_b, s_w, r_w, s_g, r_g, s_p, r_p,
           s_q1, r_q1, s_q2, r_q2, s_e, r_e, s_f, r_f):
    side = SIDE
    n_ep, n_tp = 2 * nz, side * side
    order = slot_order(nz)
    slots = n_ep
    own = 2 * order.index(0)
    assert own == 0 and sum(SIZES) == slots
    me, mt = lax.axis_index("ep"), lax.axis_index("tp")
    z, core = me // 2, lax.rem(me, 2)
    y, x = mt // side, lax.rem(mt, side)
    fh = gw.shape[1]
    nt = tokc.shape[0]

    col = pl.ds(pl.multiple_of(mt * LANES, LANES), LANES)
    load_i = pltpu.make_async_copy(ids_hbm, ids_ref, sem_i.at[0])
    load_r = pltpu.make_async_copy(rw_hbm, rw_ref, sem_i.at[1])
    load_t = pltpu.make_async_copy(tok.at[:, col], tokc, sem_tc.at[0])
    load_c = pltpu.make_async_copy(cot.at[:, col], cotc, sem_tc.at[1])
    for load in (load_i, load_r, load_t, load_c):
        load.start()

    def at(dx, dy):
        return lax.rem(y + dy, side) * side + lax.rem(x + dx, side)

    def along(axis, d):
        return at(d, 0) if axis == 0 else at(0, d)

    def far(slot):
        return lax.rem(z + order[slot // 2], nz) * 2 + lax.rem(core + slot % 2, 2)

    def back_slot(slot):
        return 2 * order.index((nz - order[slot // 2]) % nz) + slot % 2

    def rcopy(src, dst, ssem, rsem, ep, tp):
        return pltpu.make_async_remote_copy(
            src_ref=src, dst_ref=dst, send_sem=ssem, recv_sem=rsem,
            device_id={"ep": ep, "tp": tp}, device_id_type=MESH,
        )

    def got(ref, rsem):
        pltpu.make_async_copy(ref, ref, rsem).wait()

    barrier = pltpu.get_barrier_semaphore()

    def greet(i, carry):
        pl.semaphore_signal(barrier, inc=1, device_id={"ep": lax.rem(me + i, n_ep), "tp": mt}, device_id_type=MESH)
        return carry

    lax.fori_loop(1, n_ep, greet, 0)
    for d in range(1, side):
        for axis in range(2):
            pl.semaphore_signal(barrier, inc=1, device_id={"ep": me, "tp": along(axis, d)}, device_id_type=MESH)

    for b in range(n_tp):
        cols = pl.ds(b * LANES, LANES)
        pltpu.make_async_copy(gw.at[0, :, cols], wgu.at[b, pl.ds(0, fh)], sem_w).start()
        pltpu.make_async_copy(uw.at[0, :, cols], wgu.at[b, pl.ds(fh, fh)], sem_w).start()

    load_i.wait()
    load_r.wait()
    ids = [ids_ref[k : k + 1, :] for k in range(2)]
    wt = [rw_ref[k : k + 1, :].astype(F32) for k in range(2)]
    e_row = lax.broadcasted_iota(jnp.int32, (n_ep, nt), 0)
    mem = [(e_row == ids[k]).astype(F32) for k in range(2)]
    upper = (lax.broadcasted_iota(jnp.int32, (nt, nt), 0) < lax.broadcasted_iota(jnp.int32, (nt, nt), 1)).astype(BF16)
    before = dot((mem[0] + mem[1]).astype(BF16), upper)
    rank = [jnp.sum(mem[k] * before, axis=0, keepdims=True).astype(jnp.int32) for k in range(2)]
    place_of = [ids[k] * CAP + rank[k] for k in range(2)]

    def hot(k):
        return (lax.broadcasted_iota(jnp.int32, (n_ep * CAP, nt), 0) == place_of[k]).astype(F32)

    h0, h1 = hot(0), hot(1)
    pick_t = h0 + h1
    scaled_t = h0 * wt[0] + h1 * wt[1]
    load_t.wait()
    load_c.wait()
    send[:, 0] = dot(pick_t.astype(BF16), tokc[...]).astype(BF16).reshape(n_ep, CAP, LANES)
    send[:, 1] = dot(scaled_t.astype(BF16), cotc[...]).astype(BF16).reshape(n_ep, CAP, LANES)
    rows[mt, own] = send[me]
    got(wgu, sem_w)

    with jax.named_scope("bar"):
        pl.semaphore_wait(barrier, n_ep - 1 + 2 * (side - 1))

    def dispatch(chunk):
        for s in range(START[chunk], START[chunk] + SIZES[chunk]):
            if s != own:
                e = far(back_slot(s))
                rcopy(send.at[e], rows.at[mt, s], s_a, r_a.at[chunk], e, mt).start()

    dispatch(0)

    def weights_out():
        w4 = wgu.reshape(side, side, LANES, LANES)
        for d in range(1, side):
            rcopy(w4.at[:, lax.rem(x + d, side)], wx.at[side - d], s_w, r_w, me, along(0, d)).start()

    if WEIGHTS_AT < 0:
        weights_out()
    for b in range(n_tp):
        cols = pl.ds(b * LANES, LANES)
        for h in range(2):
            pltpu.make_async_copy(dw.at[0, :, cols], wd.at[b, pl.ds(h * fh, fh)], sem_wd).start()
    pickv[...] = jnp.transpose(pick_t).astype(BF16)
    got(wd, sem_wd)
    for chunk in range(1, CHUNKS):
        dispatch(chunk)

    def ref_of(q, du, dv):
        b = at(du, dv) if FIRST_AXIS[q] == 0 else at(dv, du)
        g, n = q // 2, SIZES[q // 2] // 2
        return rows.at[b, pl.ds(START[g] + q % 2 * n, n)]

    def span(g):
        return pl.ds(START[g] * CAP, SIZES[g] * CAP)

    def pass_on(q, du, dv, second, step):
        rdu, rdv = (du, (dv - step) % side) if second else ((du - step) % side, dv)
        axis = FIRST_AXIS[q] ^ int(second)
        ref = ref_of(q, du, dv)
        rcopy(ref, ref, s_b, r_b.at[(q * side + rdu) * side + rdv], me, along(axis, step % side)).start()

    def block(q, du, dv):
        got(ref_of(q, du, dv), r_b.at[(q * side + du) * side + dv])

    def both(q, du, dv, second):
        pass_on(q, du, dv, second, 1)
        pass_on(q, du, dv, second, -1)

    def relay(q, keep, second):
        step = FIRST_STEP[q] if not second else 1 if (q + keep) % 2 == 0 else -1
        v = side - 1 if step == 1 else 1
        pass_on(q, *((keep, v) if second else (v, keep)), second, step)

    def spread(q, du):
        both(q, du, 0, True)
        if q in DIRECT2:
            pass_on(q, du, 0, True, 2)

    def halves(g):
        return (2 * g, 2 * g + 1)

    def level0(g):
        skip = 1 if g == 0 else 0
        got(rows.at[mt, pl.ds(START[g] + skip, SIZES[g] - skip)], r_a.at[g])
        for q in halves(g):
            both(q, 0, 0, False)
            if q in DIRECT1:
                pass_on(q, 0, 0, False, 2)
        for q in halves(g):
            spread(q, 0)
        if g == WEIGHTS_AT:
            weights_out()

    def second_in(q, du):
        if q not in DIRECT2:
            block(q, du, 1)
            block(q, du, side - 1)
            relay(q, du, True)

    def level1(g):
        for q in halves(g):
            block(q, 1, 0)
            block(q, side - 1, 0)
            if q not in DIRECT1:
                relay(q, 0, False)
            spread(q, 1)
            spread(q, side - 1)
        for q in halves(g):
            second_in(q, 0)

    def level2(g):
        for q in halves(g):
            block(q, 2, 0)
            spread(q, 2)
        for q in halves(g):
            second_in(q, 1)
            second_in(q, side - 1)

    def level3(g):
        for q in halves(g):
            second_in(q, 2)

    def level4(g):
        for q in halves(g):
            for du in range(side):
                if q in DIRECT2:
                    block(q, du, 1)
                    block(q, du, side - 1)
                block(q, du, 2)

    def level5(g):
        per = SIZES[g]
        crows = per * CAP
        half = lax.broadcasted_iota(jnp.int32, (crows, LANES), 1) < fh
        pre = jnp.zeros((crows, LANES), F32)
        back = jnp.zeros((crows, LANES), F32)
        for b in range(0, n_tp, 2):
            a = [rows[b + i, pl.ds(START[g], per)] for i in range(2)]
            t = jnp.concatenate([a[i][:, 0].reshape(crows, LANES) for i in range(2)], axis=1)
            c = jnp.concatenate([a[i][:, 1].reshape(crows, LANES) for i in range(2)], axis=1)
            wt_b = jnp.concatenate([wgu[b], wgu[b + 1]], axis=1)
            wd_b = jnp.concatenate([wd[b], wd[b + 1]], axis=1)
            pre = pre + dot(t, wt_b, ((1,), (1,)))
            back = back + dot(c, wd_b, ((1,), (1,)))
        other = pltpu.roll(pre, fh, 1)
        gate = jnp.where(half, pre, other)
        up = jnp.where(half, other, pre)
        sig = jax.nn.sigmoid(gate)
        silu = gate * sig
        hidden = silu * up
        grad = back * jnp.where(half, up * sig * (1.0 + gate * (1.0 - sig)), silu)
        gsrc[span(g)] = grad.astype(BF16)
        hsrc[span(g)] = hidden.astype(BF16)
        prod = jnp.where(half, hidden * back, 0.0)
        if crows < LANES:
            prod = jnp.concatenate([prod, jnp.zeros((LANES - crows, LANES), F32)], axis=0)
        prod = jnp.transpose(prod)
        q0[g] = jnp.sum(prod, axis=0, keepdims=True)
        for d in range(1, side):
            rcopy(gsrc.at[span(g)], grecv.at[side - d, span(g)], s_g, r_g.at[g], me, along(0, d)).start()
        for d in range(1, side):
            rcopy(q0.at[g], q1r.at[g, side - d], s_q1, r_q1.at[g], me, along(0, d)).start()

    def level6(g):
        if g == 0:
            got(wx.at[pl.ds(1, side - 1)], r_w)
        crows = SIZES[g] * CAP
        got(grecv.at[pl.ds(1, side - 1), span(g)], r_g.at[g])
        lhs = [gsrc[span(g)]] + [grecv[r, span(g)] for r in range(1, side)]
        lhs = [jnp.concatenate(lhs[k : k + 2], axis=1) for k in range(0, side, 2)]
        for d in reversed(range(0, side, 2)):
            acc = jnp.zeros((crows, 2 * LANES), F32)
            for k in range(0, side, 2):
                parts = []
                for r in (k, k + 1):
                    w = []
                    for dd in (d, d + 1):
                        w.append(wgu[along(1, dd)] if r == 0 else wx[r, lax.rem(y + dd, side)])
                    parts.append(jnp.concatenate(w, axis=1))
                acc = acc + dot(lhs[k // 2], jnp.concatenate(parts, axis=0))
            for i, dd in enumerate((d, d + 1)):
                piece = acc[:, i * LANES : (i + 1) * LANES]
                if dd == 0:
                    pkeep[span(g)] = piece
                else:
                    psrc[dd, span(g)] = piece.astype(BF16)
        for d in range(1, side):
            rcopy(psrc.at[d, span(g)], precv.at[side - d, span(g)], s_p, r_p.at[g], me, along(1, d)).start()
        got(q1r.at[g, pl.ds(1, side - 1)], r_q1.at[g])
        q1s[g] = q0[g] + q1r[g, 1] + q1r[g, 2] + q1r[g, 3]
        for d in range(1, side):
            rcopy(q1s.at[g], q2r.at[g, side - d], s_q2, r_q2.at[g], me, along(1, d)).start()

    lane = lax.broadcasted_iota(jnp.int32, (1, LANES), 1)

    def level7(g):
        per = SIZES[g]
        got(precv.at[pl.ds(1, side - 1), span(g)], r_p.at[g])
        total = pkeep[span(g)]
        for r in range(1, side):
            total = total + precv[r, span(g)].astype(F32)
        pback[pl.ds(START[g], per)] = total.astype(BF16).reshape(per, CAP, LANES)
        for i in range(per):
            s = START[g] + i
            if s == own:
                ret[me] = pback[s]
            else:
                rcopy(pback.at[s], ret.at[me], s_e, r_e, far(s), mt).start()
        got(q2r.at[g, pl.ds(1, side - 1)], r_q2.at[g])
        qtot = q1s[g] + q2r[g, 1] + q2r[g, 2] + q2r[g, 3]
        lines = [jnp.where(lane < CAP, pltpu.roll(qtot, (LANES - CAP * i) % LANES, 1), 0.0) for i in range(per)]
        lines = pltpu.roll(jnp.concatenate(lines, axis=0), lax.rem(me, LANES // CAP) * CAP, 1)
        for i in range(per):
            qsend[START[g] + i] = lines[i : i + 1]
        for i in range(per):
            s = START[g] + i
            if s == own:
                retq[me] = qsend[s]
            else:
                rcopy(qsend.at[s], retq.at[me], s_f, r_f, far(s), mt).start()

    def weight_grads(which):
        lhs = jnp.transpose((gsrc if which == 0 else hsrc)[...].astype(F32)).astype(BF16)
        for b in range(0, n_tp, 2):
            c = jnp.concatenate([rows[b + i, :, which].reshape(slots * CAP, LANES) for i in range(2)], axis=1)
            cols = slice(b * LANES, (b + 2) * LANES)
            if which == 0:
                r = dot(lhs, c)
                gg_out[0, :, cols] = r[:fh]
                ug_out[0, :, cols] = r[fh:]
            else:
                dg_out[0, :, cols] = dot(lhs[:fh], c)

    levels = [level0, level1, level2, level3, level4, level5, level6, level7]
    last = CHUNKS - 1
    for t in range(CHUNKS + 6):
        starts = [(0, g) for g in range(CHUNKS) if t == max(0, g - AHEAD)]
        for k, g in [(4, t - 4), (3, t - 3), (2, t - 2), (1, t - 1), *starts, (5, t - 4), (6, t - 5), (7, t - 6)]:
            if 0 <= g < CHUNKS:
                if (k, g) == (6, last):
                    with jax.named_scope("wg0"):
                        weight_grads(0)
                if (k, g) == (7, last):
                    with jax.named_scope("wg1"):
                        weight_grads(1)
                with jax.named_scope(f"L{k}g{g}"):
                    levels[k](g)

    with jax.named_scope("back"):
        got(ret.at[pl.ds(0, n_ep - 1)], r_e)
    tg_out[...] = dot(pickv[...], ret[...].reshape(n_ep * CAP, LANES)).astype(BF16)
    with jax.named_scope("backq"):
        got(retq.at[pl.ds(0, n_ep - 1)], r_f)
    group = LANES // CAP
    table = jnp.concatenate([jnp.sum(retq[a * group : (a + 1) * group], axis=0) for a in range(n_ep // group)], axis=1)
    table = jnp.broadcast_to(table, (8, n_ep * CAP))
    for k in range(2):
        r = dot(table, hot(k), precision=lax.Precision.HIGHEST)
        rg_out[k : k + 1, :] = r[:1] / wt[k]

    with jax.named_scope("drain"):
        got(send.at[pl.ds(0, n_ep - 1)], s_a)
        got(rows.at[pl.ds(0, n_tp - 1)], s_b)
        got(wx.at[pl.ds(1, side - 1)], s_w)
        got(grecv.at[pl.ds(1, side - 1)], s_g)
        got(precv.at[pl.ds(1, side - 1)], s_p)
        got(q1r.at[:, pl.ds(1, side - 1)], s_q1)
        got(q2r.at[:, pl.ds(1, side - 1)], s_q2)
        got(ret.at[pl.ds(0, n_ep - 1)], s_e)
        got(retq.at[pl.ds(0, n_ep - 1)], s_f)


def write_out(n, *refs):
    copies = [pltpu.make_async_copy(refs[i], refs[n + i], refs[2 * n].at[i]) for i in range(n)]
    for c in copies:
        c.start()
    for c in copies:
        c.wait()


def per_device(nz, tokens, cotangent, expert_ids, route_weight, gate_weight, up_weight, down_weight):
    side = SIDE
    n_ep, n_tp = 2 * nz, side * side
    all_rows = n_ep * CAP
    nt = tokens.shape[0]
    fh = gate_weight.shape[1]
    vmem = pl.BlockSpec(memory_space=pltpu.VMEM)
    hbm = pl.BlockSpec(memory_space=pltpu.HBM)
    dma = pltpu.SemaphoreType.DMA
    scratch = [
        pltpu.VMEM((2, nt), jnp.int32),
        pltpu.VMEM((2, nt), BF16),
        pltpu.VMEM((nt, LANES), BF16),
        pltpu.VMEM((nt, LANES), BF16),
        pltpu.VMEM((n_tp, LANES, LANES), BF16),
        pltpu.VMEM((n_tp, LANES, LANES), BF16),
        pltpu.VMEM((n_ep, 2, CAP, LANES), BF16),
        pltpu.VMEM((n_tp, n_ep, 2, CAP, LANES), BF16),
        pltpu.VMEM((side, side, LANES, LANES), BF16),
        pltpu.VMEM((all_rows, LANES), BF16),
        pltpu.VMEM((all_rows, LANES), BF16),
        pltpu.VMEM((side, all_rows, LANES), BF16),
        pltpu.VMEM((all_rows, LANES), F32),
        pltpu.VMEM((side, all_rows, LANES), BF16),
        pltpu.VMEM((side, all_rows, LANES), BF16),
        pltpu.VMEM((n_ep, CAP, LANES), BF16),
        pltpu.VMEM((CHUNKS, 1, LANES), F32),
        pltpu.VMEM((CHUNKS, side, 1, LANES), F32),
        pltpu.VMEM((CHUNKS, 1, LANES), F32),
        pltpu.VMEM((CHUNKS, side, 1, LANES), F32),
        pltpu.VMEM((n_ep, 1, LANES), F32),
        pltpu.VMEM((n_ep, CAP, LANES), BF16),
        pltpu.VMEM((n_ep, 1, LANES), F32),
        pltpu.VMEM((nt, n_ep * CAP), BF16),
        dma((2,)), dma((2,)), dma, dma,
        dma, dma((CHUNKS,)),
        dma, dma((2 * CHUNKS * n_tp,)),
        dma, dma,
        dma, dma((CHUNKS,)),
        dma, dma((CHUNKS,)),
        dma, dma((CHUNKS,)),
        dma, dma((CHUNKS,)),
        dma, dma,
        dma, dma,
    ]
    shapes = [((nt, LANES), BF16), ((2, nt), F32)] + [(gate_weight.shape, F32)] * 3
    ins = (tokens, cotangent, expert_ids.T, route_weight.T, gate_weight, up_weight, down_weight)
    made = pl.pallas_call(
        functools.partial(kernel, nz),
        out_shape=tuple(pltpu.VMEM(*a) for a in shapes),
        in_specs=[hbm] * 7,
        out_specs=(vmem,) * 5,
        scratch_shapes=scratch,
        compiler_params=pltpu.CompilerParams(collective_id=0, has_side_effects=True, vmem_limit_bytes=24 * 1024 * 1024),
    )(*(pltpu.with_memory_space_constraint(a, pltpu.HBM) for a in ins))
    tg, rg, *grads = pl.pallas_call(
        functools.partial(write_out, 5),
        out_shape=tuple(pltpu.HBM(*a) for a in shapes),
        in_specs=[vmem] * 5,
        out_specs=(hbm,) * 5,
        scratch_shapes=[dma((5,))],
        compiler_params=pltpu.CompilerParams(vmem_limit_bytes=1024 * 1024),
    )(*(pltpu.with_memory_space_constraint(a, pltpu.VMEM) for a in made))
    return (tg, rg.T, *grads)


def solution(mesh):
    nz = mesh.shape["ep"] // 2
    in_specs = (
        P("ep", None), P("ep", None), P("ep", None), P("ep", None),
        P("ep", "tp", None), P("ep", "tp", None), P("ep", "tp", None),
    )
    out_specs = (
        P("ep", "tp"), P("ep", None), P("ep", "tp", None), P("ep", "tp", None), P("ep", "tp", None),
    )
    return jax.shard_map(
        functools.partial(per_device, nz), mesh=mesh, in_specs=in_specs, out_specs=out_specs, check_vma=False
    )
```

time: 91 us -> 73.8 us (0.81)
  local copies, waits for them, and re-layouts: 9.46 us -> 0 us
  Pallas kernels: 80.6 us -> 72.8 us
    unnamed x18 -> x0, local copies, waits for them, and re-layouts: 8.83 us -> none
    pallas_call x1 -> x2, Pallas kernels: 80.6 us -> 72.8 us  [the longest x1 71.6 us: per_device(): pl.pallas_call(functools.partial(kernel, nz), out_shape=tuple((pltpu.VMEM...]
where the time goes in v2:
time: 73.8 us; the launch traced here: 73.5 us
  Pallas kernels  72.8 us (99%)
    pallas_call x1, Pallas kernels, per_device(): pl.pallas_call(functools.partial(kernel, nz), out_shape=tuple((pltpu.VMEM...  71.6 us

profile of v2, /device:TPU:1, one launch (start us, length us, event | category | flops | bytes accessed | tf_op | source)
XLA Modules:
  0.0 73.5 jit_solution(7233613082977473865)
XLA Ops:
  0.6 71.6 %shard_map.110 = (bf16[128,128]{1,0:T(8,128)(2,1)S(1)}, f32[2,128]{1,0:T(2,128)S(1)}, f32[1,64,2048]{2,1,0:T(8,128)S(1)}, f32[1,64,2048]{2,1,0:T(8,128)S(1)}, f32[1,64,2048]{2,1,0:T(8,128)S(1)}) custom-call(bf16[128,2048]{1,0:T(8,128)(2,1)} %tok.1, bf16[128,2048]{1,0:T(8,128)(2,1)} %cot.1, s32[2,128]{1,0:T(2,128)} %bitcast.3, bf16[2,128]{1,0:T(2,128)(2,1)} %bitcast.4, ...), custom_call_target="tpu_custom_call" | custom-call | tf_op jit(solution)/shard_map/pallas_call | solution.py:431
  72.3 1.2 %shard_map.111 = (bf16[128,128]{1,0:T(8,128)(2,1)}, f32[2,128]{1,0:T(2,128)}, f32[1,64,2048]{2,1,0:T(8,128)}, f32[1,64,2048]{2,1,0:T(8,128)}, f32[1,64,2048]{2,1,0:T(8,128)}) custom-call(bf16[128,128]{1,0:T(8,128)(2,1)S(1)} %get-tuple-element.15.refs_0_, f32[2,128]{1,0:T(2,128)S(1)} %get-tuple-element.16.refs_1_, ...), custom_call_target="tpu_custom_call" | custom-call | tf_op jit(solution)/shard_map/pallas_call | solution.py:439

commit v3 on v2

--- a/solution.py
+++ b/solution.py
@@ -24,15 +24,19 @@
 def slot_order(nz):
     near = [0] + [d for k in range(1, nz // 2) for d in (k, nz - k)] + [nz // 2]
     n = nz // 4
-    return near[:n] + near[2 * n :] + near[n : 2 * n]
+    return near[:n] + near[2 * n : 3 * n] + near[n : 2 * n] + near[3 * n :]
 
 
 FIRST_AXIS = (0, 1) * CHUNKS
 FIRST_STEP = (1, 1, -1, -1) * CHUNKS
 DIRECT1 = tuple(range(2 * CHUNKS))
+XPART = (4, 4, 4, 4)
 DIRECT2 = ()
-WEIGHTS_AT = -1
-AHEAD = 0
+WPARTS, WFIRST = 1, 1
+PROGRAM = (
+    (0, 0), (1, 0), (0, 1), (2, 0), (1, 1), (0, 3), (3, 0), (2, 1), (1, 3), (0, 2), (5, 0), (3, 1), (2, 3), (1, 2), (5, 1),
+    (6, 0), (3, 3), (5, 3), (2, 2), (6, 1), (7, 0), (6, 3), (3, 2), (5, 2), (7, 1), (8, 0), (7, 3), (6, 2), (8, 1), (7, 2),
+)
 
 
 def kernel(nz, tok, cot, ids_hbm, rw_hbm, gw, uw, dw, tg_out, rg_out, gg_out, ug_out, dg_out,
@@ -45,7 +49,7 @@
     order = slot_order(nz)
     slots = n_ep
     own = 2 * order.index(0)
-    assert own == 0 and sum(SIZES) == slots
+    assert own in START and sum(SIZES) == slots
     me, mt = lax.axis_index("ep"), lax.axis_index("tp")
     z, core = me // 2, lax.rem(me, 2)
     y, x = mt // side, lax.rem(mt, side)
@@ -132,26 +136,28 @@
 
     dispatch(0)
 
-    def weights_out():
+    def weights_out(part):
         w4 = wgu.reshape(side, side, LANES, LANES)
+        some = pl.ds(part * side // WPARTS, side // WPARTS)
         for d in range(1, side):
-            rcopy(w4.at[:, lax.rem(x + d, side)], wx.at[side - d], s_w, r_w, me, along(0, d)).start()
-
-    if WEIGHTS_AT < 0:
-        weights_out()
+            rcopy(w4.at[some, lax.rem(x + d, side)], wx.at[side - d, some], s_w, r_w, me, along(0, d)).start()
+
+    for part in range(WFIRST):
+        weights_out(part)
     for b in range(n_tp):
         cols = pl.ds(b * LANES, LANES)
         for h in range(2):
             pltpu.make_async_copy(dw.at[0, :, cols], wd.at[b, pl.ds(h * fh, fh)], sem_wd).start()
     pickv[...] = jnp.transpose(pick_t).astype(BF16)
     got(wd, sem_wd)
-    for chunk in range(1, CHUNKS):
+    for chunk in (1, 3, 2):
         dispatch(chunk)
 
     def ref_of(q, du, dv):
         b = at(du, dv) if FIRST_AXIS[q] == 0 else at(dv, du)
-        g, n = q // 2, SIZES[q // 2] // 2
-        return rows.at[b, pl.ds(START[g] + q % 2 * n, n)]
+        g = q // 2
+        n = XPART[g]
+        return rows.at[b, pl.ds(START[g] + n, SIZES[g] - n) if q % 2 else pl.ds(START[g], n)]
 
     def span(g):
         return pl.ds(START[g] * CAP, SIZES[g] * CAP)
@@ -183,7 +189,7 @@
         return (2 * g, 2 * g + 1)
 
     def level0(g):
-        skip = 1 if g == 0 else 0
+        skip = 1 if START[g] == own else 0
         got(rows.at[mt, pl.ds(START[g] + skip, SIZES[g] - skip)], r_a.at[g])
         for q in halves(g):
             both(q, 0, 0, False)
@@ -191,8 +197,6 @@
                 pass_on(q, 0, 0, False, 2)
         for q in halves(g):
             spread(q, 0)
-        if g == WEIGHTS_AT:
-            weights_out()
 
     def second_in(q, du):
         if q not in DIRECT2:
@@ -202,28 +206,21 @@
 
     def level1(g):
         for q in halves(g):
-            block(q, 1, 0)
-            block(q, side - 1, 0)
+            for du in (1, side - 1):
+                block(q, du, 0)
+                spread(q, du)
             if q not in DIRECT1:
                 relay(q, 0, False)
-            spread(q, 1)
-            spread(q, side - 1)
-        for q in halves(g):
-            second_in(q, 0)
-
-    def level2(g):
         for q in halves(g):
             block(q, 2, 0)
             spread(q, 2)
-        for q in halves(g):
-            second_in(q, 1)
-            second_in(q, side - 1)
+
+    def level2(g):
+        for du in (0, 1, side - 1, 2):
+            for q in halves(g):
+                second_in(q, du)
 
     def level3(g):
-        for q in halves(g):
-            second_in(q, 2)
-
-    def level4(g):
         for q in halves(g):
             for du in range(side):
                 if q in DIRECT2:
@@ -268,6 +265,10 @@
         if g == 0:
             got(wx.at[pl.ds(1, side - 1)], r_w)
         crows = SIZES[g] * CAP
+        got(q1r.at[g, pl.ds(1, side - 1)], r_q1.at[g])
+        q1s[g] = q0[g] + q1r[g, 1] + q1r[g, 2] + q1r[g, 3]
+        for d in range(1, side):
+            rcopy(q1s.at[g], q2r.at[g, side - d], s_q2, r_q2.at[g], me, along(1, d)).start()
         got(grecv.at[pl.ds(1, side - 1), span(g)], r_g.at[g])
         lhs = [gsrc[span(g)]] + [grecv[r, span(g)] for r in range(1, side)]
         lhs = [jnp.concatenate(lhs[k : k + 2], axis=1) for k in range(0, side, 2)]
@@ -289,26 +290,11 @@
                     psrc[dd, span(g)] = piece.astype(BF16)
         for d in range(1, side):
             rcopy(psrc.at[d, span(g)], precv.at[side - d, span(g)], s_p, r_p.at[g], me, along(1, d)).start()
-        got(q1r.at[g, pl.ds(1, side - 1)], r_q1.at[g])
-        q1s[g] = q0[g] + q1r[g, 1] + q1r[g, 2] + q1r[g, 3]
-        for d in range(1, side):
-            rcopy(q1s.at[g], q2r.at[g, side - d], s_q2, r_q2.at[g], me, along(1, d)).start()
 
     lane = lax.broadcasted_iota(jnp.int32, (1, LANES), 1)
 
     def level7(g):
         per = SIZES[g]
-        got(precv.at[pl.ds(1, side - 1), span(g)], r_p.at[g])
-        total = pkeep[span(g)]
-        for r in range(1, side):
-            total = total + precv[r, span(g)].astype(F32)
-        pback[pl.ds(START[g], per)] = total.astype(BF16).reshape(per, CAP, LANES)
-        for i in range(per):
-            s = START[g] + i
-            if s == own:
-                ret[me] = pback[s]
-            else:
-                rcopy(pback.at[s], ret.at[me], s_e, r_e, far(s), mt).start()
         got(q2r.at[g, pl.ds(1, side - 1)], r_q2.at[g])
         qtot = q1s[g] + q2r[g, 1] + q2r[g, 2] + q2r[g, 3]
         lines = [jnp.where(lane < CAP, pltpu.roll(qtot, (LANES - CAP * i) % LANES, 1), 0.0) for i in range(per)]
@@ -321,6 +307,17 @@
                 retq[me] = qsend[s]
             else:
                 rcopy(qsend.at[s], retq.at[me], s_f, r_f, far(s), mt).start()
+        got(precv.at[pl.ds(1, side - 1), span(g)], r_p.at[g])
+        total = pkeep[span(g)]
+        for r in range(1, side):
+            total = total + precv[r, span(g)].astype(F32)
+        pback[pl.ds(START[g], per)] = total.astype(BF16).reshape(per, CAP, LANES)
+        for i in range(per):
+            s = START[g] + i
+            if s == own:
+                ret[me] = pback[s]
+            else:
+                rcopy(pback.at[s], ret.at[me], s_e, r_e, far(s), mt).start()
 
     def weight_grads(which):
         lhs = jnp.transpose((gsrc if which == 0 else hsrc)[...].astype(F32)).astype(BF16)
@@ -334,24 +331,11 @@
             else:
                 dg_out[0, :, cols] = dot(lhs[:fh], c)
 
-    levels = [level0, level1, level2, level3, level4, level5, level6, level7]
-    last = CHUNKS - 1
-    for t in range(CHUNKS + 6):
-        starts = [(0, g) for g in range(CHUNKS) if t == max(0, g - AHEAD)]
-        for k, g in [(4, t - 4), (3, t - 3), (2, t - 2), (1, t - 1), *starts, (5, t - 4), (6, t - 5), (7, t - 6)]:
-            if 0 <= g < CHUNKS:
-                if (k, g) == (6, last):
-                    with jax.named_scope("wg0"):
-                        weight_grads(0)
-                if (k, g) == (7, last):
-                    with jax.named_scope("wg1"):
-                        weight_grads(1)
-                with jax.named_scope(f"L{k}g{g}"):
-                    levels[k](g)
-
-    with jax.named_scope("back"):
-        got(ret.at[pl.ds(0, n_ep - 1)], r_e)
-    tg_out[...] = dot(pickv[...], ret[...].reshape(n_ep * CAP, LANES)).astype(BF16)
+    levels = {0: level0, 1: level1, 2: level2, 3: level3, 5: level5, 6: level6, 7: level7, 8: weight_grads, 9: weights_out}
+    for k, g in PROGRAM:
+        with jax.named_scope(f"L{k}g{g}"):
+            levels[k](g)
+
     with jax.named_scope("backq"):
         got(retq.at[pl.ds(0, n_ep - 1)], r_f)
     group = LANES // CAP
@@ -360,6 +344,10 @@
     for k in range(2):
         r = dot(table, hot(k), precision=lax.Precision.HIGHEST)
         rg_out[k : k + 1, :] = r[:1] / wt[k]
+
+    with jax.named_scope("back"):
+        got(ret.at[pl.ds(0, n_ep - 1)], r_e)
+    tg_out[...] = dot(pickv[...], ret[...].reshape(n_ep * CAP, LANES)).astype(BF16)
 
     with jax.named_scope("drain"):
         got(send.at[pl.ds(0, n_ep - 1)], s_a)

time: 73.8 us -> 73.1 us (level)
  no operation moved by 1% of the time
where the time goes in v3:
time: 73.1 us; the launch traced here: 72.8 us
  Pallas kernels  72.2 us (99%)
    pallas_call x1, Pallas kernels, per_device(): pl.pallas_call(functools.partial(kernel, nz), out_shape=tuple((pltpu.VMEM...  71 us

profile of v3, /device:TPU:1, one launch (start us, length us, event | category | flops | bytes accessed | tf_op | source)
XLA Modules:
  0.0 72.8 jit_solution(1751954475619591088)
XLA Ops:
  0.6 71.0 %shard_map.110 = (bf16[128,128]{1,0:T(8,128)(2,1)S(1)}, f32[2,128]{1,0:T(2,128)S(1)}, f32[1,64,2048]{2,1,0:T(8,128)S(1)}, f32[1,64,2048]{2,1,0:T(8,128)S(1)}, f32[1,64,2048]{2,1,0:T(8,128)S(1)}) custom-call(bf16[128,2048]{1,0:T(8,128)(2,1)} %tok.1, bf16[128,2048]{1,0:T(8,128)(2,1)} %cot.1, s32[2,128]{1,0:T(2,128)} %bitcast.3, bf16[2,128]{1,0:T(2,128)(2,1)} %bitcast.4, ...), custom_call_target="tpu_custom_call" | custom-call | tf_op jit(solution)/shard_map/pallas_call | solution.py:419
  71.6 1.2 %shard_map.111 = (bf16[128,128]{1,0:T(8,128)(2,1)}, f32[2,128]{1,0:T(2,128)}, f32[1,64,2048]{2,1,0:T(8,128)}, f32[1,64,2048]{2,1,0:T(8,128)}, f32[1,64,2048]{2,1,0:T(8,128)}) custom-call(bf16[128,128]{1,0:T(8,128)(2,1)S(1)} %get-tuple-element.15.refs_0_, f32[2,128]{1,0:T(2,128)S(1)} %get-tuple-element.16.refs_1_, ...), custom_call_target="tpu_custom_call" | custom-call | tf_op jit(solution)/shard_map/pallas_call | solution.py:427

commit v4 on v3

--- a/solution.py
+++ b/solution.py
@@ -30,7 +30,7 @@
 FIRST_AXIS = (0, 1) * CHUNKS
 FIRST_STEP = (1, 1, -1, -1) * CHUNKS
 DIRECT1 = tuple(range(2 * CHUNKS))
-XPART = (4, 4, 4, 4)
+XPART = (4, 5, 5, 5)
 DIRECT2 = ()
 WPARTS, WFIRST = 1, 1
 PROGRAM = (

time: 73.1 us -> 71.9 us (0.984)
  Pallas kernels: 72.2 us -> 70.9 us
    pallas_call x1, Pallas kernels: 71 us -> 69.7 us  [per_device(): pl.pallas_call(functools.partial(kernel, nz), out_shape=tuple((pltpu.VMEM...]
where the time goes in v4:
time: 71.9 us; the launch traced here: 71.6 us
  Pallas kernels  70.9 us (99%)
    pallas_call x1, Pallas kernels, per_device(): pl.pallas_call(functools.partial(kernel, nz), out_shape=tuple((pltpu.VMEM...  69.7 us

profile of v4, /device:TPU:1, one launch (start us, length us, event | category | flops | bytes accessed | tf_op | source)
XLA Modules:
  0.0 71.6 jit_solution(16011786792225946310)
XLA Ops:
  0.6 69.7 %shard_map.110 = (bf16[128,128]{1,0:T(8,128)(2,1)S(1)}, f32[2,128]{1,0:T(2,128)S(1)}, f32[1,64,2048]{2,1,0:T(8,128)S(1)}, f32[1,64,2048]{2,1,0:T(8,128)S(1)}, f32[1,64,2048]{2,1,0:T(8,128)S(1)}) custom-call(bf16[128,2048]{1,0:T(8,128)(2,1)} %tok.1, bf16[128,2048]{1,0:T(8,128)(2,1)} %cot.1, s32[2,128]{1,0:T(2,128)} %bitcast.3, bf16[2,128]{1,0:T(2,128)(2,1)} %bitcast.4, ...), custom_call_target="tpu_custom_call" | custom-call | tf_op jit(solution)/shard_map/pallas_call | solution.py:419
  70.4 1.2 %shard_map.111 = (bf16[128,128]{1,0:T(8,128)(2,1)}, f32[2,128]{1,0:T(2,128)}, f32[1,64,2048]{2,1,0:T(8,128)}, f32[1,64,2048]{2,1,0:T(8,128)}, f32[1,64,2048]{2,1,0:T(8,128)}) custom-call(bf16[128,128]{1,0:T(8,128)(2,1)S(1)} %get-tuple-element.15.refs_0_, f32[2,128]{1,0:T(2,128)S(1)} %get-tuple-element.16.refs_1_, ...), custom_call_target="tpu_custom_call" | custom-call | tf_op jit(solution)/shard_map/pallas_call | solution.py:427

commit v5 on v4

--- a/solution.py
+++ b/solution.py
@@ -205,7 +205,7 @@
             relay(q, du, True)
 
     def level1(g):
-        for q in halves(g):
+        for q in reversed(halves(g)) if g == 0 else halves(g):
             for du in (1, side - 1):
                 block(q, du, 0)
                 spread(q, du)

time: 71.9 us -> 71.9 us (level)
  no operation moved by 1% of the time
where the time goes in v5:
time: 71.9 us; the launch traced here: 71.6 us
  Pallas kernels  71 us (99%)
    pallas_call x1, Pallas kernels, per_device(): pl.pallas_call(functools.partial(kernel, nz), out_shape=tuple((pltpu.VMEM...  69.8 us

profile of v5, /device:TPU:1, one launch (start us, length us, event | category | flops | bytes accessed | tf_op | source)
XLA Modules:
  0.0 71.6 jit_solution(12906190073921696801)
XLA Ops:
  0.6 69.8 %shard_map.110 = (bf16[128,128]{1,0:T(8,128)(2,1)S(1)}, f32[2,128]{1,0:T(2,128)S(1)}, f32[1,64,2048]{2,1,0:T(8,128)S(1)}, f32[1,64,2048]{2,1,0:T(8,128)S(1)}, f32[1,64,2048]{2,1,0:T(8,128)S(1)}) custom-call(bf16[128,2048]{1,0:T(8,128)(2,1)} %tok.1, bf16[128,2048]{1,0:T(8,128)(2,1)} %cot.1, s32[2,128]{1,0:T(2,128)} %bitcast.3, bf16[2,128]{1,0:T(2,128)(2,1)} %bitcast.4, ...), custom_call_target="tpu_custom_call" | custom-call | tf_op jit(solution)/shard_map/pallas_call | solution.py:419
  70.4 1.2 %shard_map.111 = (bf16[128,128]{1,0:T(8,128)(2,1)}, f32[2,128]{1,0:T(2,128)}, f32[1,64,2048]{2,1,0:T(8,128)}, f32[1,64,2048]{2,1,0:T(8,128)}, f32[1,64,2048]{2,1,0:T(8,128)}) custom-call(bf16[128,128]{1,0:T(8,128)(2,1)S(1)} %get-tuple-element.15.refs_0_, f32[2,128]{1,0:T(2,128)S(1)} %get-tuple-element.16.refs_1_, ...), custom_call_target="tpu_custom_call" | custom-call | tf_op jit(solution)/shard_map/pallas_call | solution.py:427
